TPU v7x, 32 devices: a whole 2x2x4 slice. The times are simulated.
32 devices in a mesh: fs: 16 (over z, y, x), tp: 2 (over core).
Axes of the slice: x: 2, y: 2, z: 4, core: 2. Of those that a mesh axis runs over, the one named last changes fastest.
Arguments:
- tokens: bfloat16 [12288, 2048], P('fs'), may hold values from -6 to 6
- norm_gain: float32 [2048], replicated, may hold values from 0.1 to 1.9
- gate_weight: bfloat16 [2048, 5120], P('fs', 'tp'), may hold values from -0.125 to 0.125
- up_weight: bfloat16 [2048, 5120], P('fs', 'tp'), may hold values from -0.125 to 0.125
- down_weight: bfloat16 [5120, 2048], P('tp', 'fs'), may hold values from -0.078125 to 0.078125
Outputs:
- mixed: bfloat16 [12288, 2048], P(('fs', 'tp'))
All inputs are finite; a program needn't handle non-finite values.
Results may differ from a plain program's by a relative error of at most 0.014.
Values may be sent and summed in bfloat16 or wider, within the bound.
A program may use at most 128 MiB of HBM per device.

v0:
```python
import jax
import jax.numpy as jnp
from jax import lax
from jax.sharding import PartitionSpec as P


def add_rows(normed, piece):
    return jnp.dot(normed, piece, preferred_element_type=jnp.float32)


def per_device(tokens, norm_gain, gate_weight, up_weight, down_weight):
    values = tokens.astype(jnp.float32)
    scale = lax.rsqrt(jnp.mean(values * values, axis=-1, keepdims=True) + 1e-06)
    normed = (values * scale * norm_gain).astype(jnp.bfloat16)

    def add_single(piece):
        return add_rows(normed, piece)

    gate_proj = add_single(lax.all_gather(gate_weight, "fs", axis=0, tiled=True))
    up_proj = add_single(lax.all_gather(up_weight, "fs", axis=0, tiled=True))
    hidden = (jax.nn.silu(gate_proj) * up_proj).astype(jnp.bfloat16)
    down_whole = lax.all_gather(down_weight, "fs", axis=1, tiled=True)
    return lax.psum_scatter(
        jnp.dot(hidden, down_whole, preferred_element_type=jnp.float32).astype(jnp.bfloat16),
        "tp",
        scatter_dimension=0,
        tiled=True,
    )


def solution(mesh):
    in_specs = (P("fs", None), P(), P("fs", "tp"), P("fs", "tp"), P("tp", "fs"))
    out_specs = P(("fs", "tp"), None)
    return jax.shard_map(
        per_device, mesh=mesh, in_specs=in_specs, out_specs=out_specs, check_vma=False
    )
```

profile of v0, /device:TPU:1, one launch (start us, length us, event | category | flops | bytes accessed | tf_op | source)
XLA Modules:
  0.0 489.7 jit_solution(3628427633222220995)
XLA Ops:
  6.5 0.0 all-gather.4.cloned.1.call-start
  6.5 0.7 all-gather.4.cloned.1.call-update
  7.3 0.0 all-gather.6.cloned.1.call-start
  7.3 0.7 all-gather.6.cloned.1.call-update
  8.0 0.0 all-gather.8.cloned.1.call-start
  8.1 0.7 all-gather.8.cloned.1.call-update
  8.7 0.0 reduce-scatter.2.cloned.1.call-start
  8.8 2.6 fusion
  11.4 0.0 copy-start
  11.4 0.0 copy-start.1
  11.4 131.1 %all-gather.4.cloned.1.call-done = bf16[2048,2560]{1,0:T(8,128)(2,1)} async-done(((bf16[128,2560]{1,0:T(8,128)(2,1)}), bf16[2048,2560]{1,0:T(8,128)(2,1)}) %all-gather.4.cloned.1.call-update) | async-done | bytes 10485776 | tf_op jit(solution)/shard_map/all_gather | solution.py:19
  142.5 13.9 %fusion.5 = f32[768,2560]{1,0:T(8,128)} fusion(bf16[2048,2560]{1,0:T(8,128)(2,1)} %all-gather.4.cloned.1.call-done, bf16[768,2048]{1,0:T(8,128)(2,1)} %param.5, f32[2048]{0:T(1024)} %param.6, f32[768]{0:T(1024)S(1)} %add_rsqrt_fusion), kind=kOutput, calls=%fused_computation.7 | convolution fusion | flops 8059355136 | bytes 21507072 | tf_op jit(solution)/shard_map/dot_general | solution.py:8
  156.4 118.4 %all-gather.6.cloned.1.call-done = bf16[2048,2560]{1,0:T(8,128)(2,1)} async-done(((bf16[128,2560]{1,0:T(8,128)(2,1)}), bf16[2048,2560]{1,0:T(8,128)(2,1)}) %all-gather.6.cloned.1.call-update) | async-done | bytes 10485776 | tf_op jit(solution)/shard_map/all_gather | solution.py:20
  274.8 170.0 %all-gather.8.cloned.1.call-done = bf16[2560,2048]{1,0:T(8,128)(2,1)} async-done(((bf16[2560,128]{1,0:T(8,128)(2,1)}), bf16[2560,2048]{1,0:T(8,128)(2,1)}) %all-gather.8.cloned.1.call-update) | async-done | bytes 10485776 | tf_op jit(solution)/shard_map/all_gather | solution.py:22
  444.8 0.0 copy-done
  444.8 0.0 copy-done.1
  444.8 27.6 %convolution_convert_fusion = bf16[768,2048]{1,0:T(8,128)(2,1)} fusion(bf16[2560,2048]{1,0:T(8,128)(2,1)} %all-gather.8.cloned.1.call-done, f32[768,2560]{1,0:T(8,128)} %fusion.5, bf16[2048,2560]{1,0:T(8,128)(2,1)} %all-gather.6.cloned.1.call-done, bf16[768,2048]{1,0:T(8,128)(2,1)S(1)} %copy-done, f32[2048]{0:T(1024)S(1)} %copy-done.1, ...), kind=kOutput, calls=%fused_computation.6 | convolution fusion | flops 16125788160 | bytes 35138560 | tf_op jit(solution)/shard_map/dot_general | solution.py:24
  472.4 0.0 reduce-scatter.2.cloned.1.call-update
  472.4 10.7 %reduce-scatter.2.cloned.1.call-done = bf16[384,2048]{1,0:T(8,128)(2,1)} async-done(((bf16[768,2048]{1,0:T(8,128)(2,1)}), bf16[384,2048]{1,0:T(8,128)(2,1)}) %reduce-scatter.2.cloned.1.call-update) | async-done | bytes 1572880 | tf_op jit(solution)/shard_map/reduce_scatter | solution.py:23
  (1 shorter events, 0.0 us)
Async XLA Ops:
  6.5 135.9 %all-gather.4.cloned.1.call-start = ((), (), s32[]{:S(2)}) async-start(), calls=%async_computation.1 | async-start | bytes 11141120 | tf_op jit(solution)/shard_map/all_gather | solution.py:19
  7.3 267.6 %all-gather.6.cloned.1.call-start = ((), (), s32[]{:S(2)}) async-start(), calls=%async_computation.2 | async-start | bytes 11141120 | tf_op jit(solution)/shard_map/all_gather | solution.py:20
  8.0 436.8 %all-gather.8.cloned.1.call-start = ((), (), s32[]{:S(2)}) async-start(), calls=%async_computation.3 | async-start | bytes 11141120 | tf_op jit(solution)/shard_map/all_gather | solution.py:22
  8.7 474.4 %reduce-scatter.2.cloned.1.call-start = ((), (), s32[]{:S(2)}) async-start(), calls=%async_computation.4 | async-start | bytes 4718592 | tf_op jit(solution)/shard_map/reduce_scatter | solution.py:23
  11.4 433.4 %copy-start = (bf16[768,2048]{1,0:T(8,128)(2,1)S(1)}, bf16[768,2048]{1,0:T(8,128)(2,1)}, u32[]{:S(2)}) copy-start(bf16[768,2048]{1,0:T(8,128)(2,1)} %param.5) | copy-start | bytes 9437188
  11.4 433.4 %copy-start.1 = (f32[2048]{0:T(1024)S(1)}, f32[2048]{0:T(1024)}, u32[]{:S(2)}) copy-start(f32[2048]{0:T(1024)} %param.6) | copy-start | bytes 24580
Sparse Core Ops, SparseCore 0:
  10.0 132.3 all-gather.3
  145.1 129.6 all-gather.5
  277.5 167.2 all-gather.7
  472.6 10.5 reduce-scatter.1
where the time goes:
time: 490 us
  waiting for transfers between devices  432 us (88%)
  matrix products  41.5 us (8%)
  between operations  13.1 us (3%)
    all_gather x1, waiting for transfers between devices, per_device(): down_whole = lax.all_gather(down_weight, 'fs', axis=1, tiled=True)  170 us
    all_gather x1, waiting for transfers between devices, per_device(): lax.all_gather(gate_weight, 'fs', axis=0, tiled=True)  131 us
    all_gather x1, waiting for transfers between devices, per_device(): up_proj = add_single(lax.all_gather(up_weight, 'fs', axis=0, tiled=True))  118 us
    dot_general x1, matrix products, per_device(): jnp.dot(hidden, down_whole, preferred_element_type=jnp.float32)  27.6 us
    dot_general x1, matrix products, add_rows(): return jnp.dot(normed, piece, preferred_element_type=jnp.float32)  13.9 us
    reduce_scatter x1, waiting for transfers between devices, per_device(): lax.psum_scatter(jnp.dot(hidden, down_whole, preferred_element_type=jnp.f...  10.7 us
  transfers between devices with their start and end apart: 4, of which 4 were waited for; matrix products, arithmetic and copies ran while one was open for 3% of the time, Pallas kernels for 0%

commit v1 on v0

v1 whole, which is shorter than its diff:
```python
import functools

import jax
import jax.numpy as jnp
from jax import lax
from jax.experimental import pallas as pl
from jax.experimental.pallas import tpu as pltpu
from jax.sharding import PartitionSpec as P

MESH = pl.DeviceIdType.MESH
PLANE = 4
ORDER = ((1, 1), (0, 1), (1, 0), (0, 0))


def simple(tokens, norm_gain, gate_weight, up_weight, down_weight):
    values = tokens.astype(jnp.float32)
    scale = lax.rsqrt(jnp.mean(values * values, axis=-1, keepdims=True) + 1e-06)
    normed = (values * scale * norm_gain).astype(jnp.bfloat16)

    def project(piece):
        whole = lax.all_gather(piece, "fs", axis=0, tiled=True)
        return jnp.dot(normed, whole, preferred_element_type=jnp.float32)

    hidden = (jax.nn.silu(project(gate_weight)) * project(up_weight)).astype(jnp.bfloat16)
    down_whole = lax.all_gather(down_weight, "fs", axis=1, tiled=True)
    return lax.psum_scatter(
        jnp.dot(hidden, down_whole, preferred_element_type=jnp.float32).astype(jnp.bfloat16),
        "tp",
        scatter_dimension=0,
        tiled=True,
    )


def kernel(nz, tok_hbm, gain_ref, gate_hbm, up_hbm, down_hbm, out_ref,
           tok, normed, gu, dn, hidden, psend, precv, own,
           loc_sem, a2a_s, a2a_r, tok_s, tok_r, up_s, dn_s, z_r, sib_s, sib_r, rs_s, rs_r):
    f = lax.axis_index("fs")
    c = lax.axis_index("tp")
    z, p = f // PLANE, f % PLANE
    y, x = p // 2, p % 2
    depth = gate_hbm.shape[0]
    width = gate_hbm.shape[1] // PLANE
    rows = tok_hbm.shape[0] // 2
    unit = depth * PLANE

    def member(k):
        oy, ox = ORDER[k]
        return ((y + oy) % 2) * 2 + (x + ox) % 2

    def dev(plane, z_, core):
        return (z_ * PLANE + plane, core)

    barrier = pltpu.get_barrier_semaphore()
    for k in range(3):
        pl.semaphore_signal(barrier, inc=1, device_id=dev(member(k), z, c), device_id_type=MESH)
    pl.semaphore_signal(barrier, inc=1, device_id=(f, 1 - c), device_id_type=MESH)

    @pl.when(z > 0)
    def _():
        pl.semaphore_signal(barrier, inc=1, device_id=dev(p, z - 1, c), device_id_type=MESH)

    @pl.when(z < nz - 1)
    def _():
        pl.semaphore_signal(barrier, inc=1, device_id=dev(p, z + 1, c), device_id_type=MESH)

    pl.semaphore_wait(barrier, 4 + (z + nz - 1) // nz + (2 * nz - 2 - z) // nz)

    sources = (gate_hbm, up_hbm, down_hbm)

    def piece_src(m, q):
        start = pl.multiple_of(q * width, 128)
        if m < 2:
            return sources[m].at[:, pl.ds(start, width)]
        return sources[m].at[pl.ds(start, width), :]

    def weight_dst(m, start, size):
        start = pl.multiple_of(start, 128)
        units = pl.ds(pl.multiple_of(c * width, 128), width)
        if m < 2:
            return gu.at[m, pl.ds(start, size), units]
        return dn.at[units, pl.ds(start, size)]

    def weight_sib(m, start, size):
        start = pl.multiple_of(start, 128)
        units = pl.ds(pl.multiple_of((1 - c) * width, 128), width)
        if m < 2:
            return gu.at[m, pl.ds(start, size), units]
        return dn.at[units, pl.ds(start, size)]

    def a2a(m, k):
        q = member(k)
        return pltpu.make_async_remote_copy(
            src_ref=piece_src(m, q), dst_ref=weight_dst(m, f * depth, depth),
            send_sem=a2a_s.at[m, k], recv_sem=a2a_r.at[m, k],
            device_id=dev(q, z, c), device_id_type=MESH)

    def a2a_in(m, k):
        q = member(k)
        ref = weight_dst(m, (z * PLANE + q) * depth, depth)
        return pltpu.make_async_remote_copy(
            src_ref=ref, dst_ref=ref, send_sem=a2a_s.at[m, k], recv_sem=a2a_r.at[m, k],
            device_id=dev(q, z, c), device_id_type=MESH)

    def local(m):
        return pltpu.make_async_copy(piece_src(m, p), weight_dst(m, f * depth, depth), loc_sem.at[m])

    half = pl.ds(pl.multiple_of(c * rows, 16), rows)

    def tok_copy(k):
        q = member(k)
        return pltpu.make_async_remote_copy(
            src_ref=tok_hbm.at[half, :], dst_ref=tok.at[k],
            send_sem=tok_s.at[k], recv_sem=tok_r.at[k],
            device_id=dev(q, z, c), device_id_type=MESH)

    own_tok = pltpu.make_async_copy(tok_hbm.at[half, :], tok.at[3], loc_sem.at[3])

    def along(m, zs, step):
        ref = weight_dst(m, zs * unit, unit)
        sems = up_s if step > 0 else dn_s
        return pltpu.make_async_remote_copy(
            src_ref=ref, dst_ref=ref, send_sem=sems.at[m, zs], recv_sem=z_r.at[m, zs],
            device_id=dev(p, z + step, c), device_id_type=MESH)

    def to_sibling(m, zs):
        ref = weight_dst(m, zs * unit, unit)
        return pltpu.make_async_remote_copy(
            src_ref=ref, dst_ref=ref, send_sem=sib_s.at[m, zs], recv_sem=sib_r.at[m, zs],
            device_id=(f, 1 - c), device_id_type=MESH)

    def from_sibling(m, zs):
        ref = weight_sib(m, zs * unit, unit)
        return pltpu.make_async_remote_copy(
            src_ref=ref, dst_ref=ref, send_sem=sib_s.at[m, zs], recv_sem=sib_r.at[m, zs],
            device_id=(f, 1 - c), device_id_type=MESH)

    def forward(m, zs):
        @pl.when((zs <= z) & (z < nz - 1))
        def _():
            along(m, zs, 1).start()

        @pl.when((zs >= z) & (z > 0))
        def _():
            along(m, zs, -1).start()

        to_sibling(m, zs).start()

    def arrived(m, zs):
        along(m, zs, 1).wait_recv()

    for m in range(3):
        for k in range(3):
            a2a(m, k).start()
        local(m).start()
    for k in range(3):
        tok_copy(k).start()
    own_tok.start()

    def own_unit(m):
        local(m).wait()
        for k in range(3):
            a2a_in(m, k).wait_recv()
        forward(m, z)

    own_unit(0)
    own_unit(1)
    for d in range(1, nz):
        for m in range(2):
            @pl.when(z - d >= 0)
            def _():
                arrived(m, z - d)
                forward(m, z - d)

            @pl.when(z + d < nz)
            def _():
                arrived(m, z + d)
                forward(m, z + d)
    own_unit(2)
    inner = (z > 0) & (z < nz - 1)
    for d in range(1, nz):
        @pl.when(inner & (z - d >= 0))
        def _():
            arrived(2, z - d)
            forward(2, z - d)

        @pl.when(inner & (z + d < nz))
        def _():
            arrived(2, z + d)
            forward(2, z + d)

    for m in range(2):
        for zs in range(nz):
            from_sibling(m, zs).wait_recv()

    def make_hidden(k):
        if k == 3:
            own_tok.wait()
        else:
            tok_copy(k).wait_recv()
        block = rows // 6

        @pl.loop(0, 6)
        def _(i):
            at = pl.ds(pl.multiple_of(i * block, 16), block)
            values = tok[k, at, :].astype(jnp.float32)
            scale = lax.rsqrt(jnp.mean(values * values, axis=-1, keepdims=True) + 1e-06)
            normed[at, :] = (values * scale * gain_ref[...]).astype(jnp.bfloat16)

        @pl.loop(0, 2 * width // 256)
        def _(j):
            at = pl.ds(pl.multiple_of(j * 256, 256), 256)
            gate = jnp.dot(normed[...], gu[0, :, at], preferred_element_type=jnp.float32)
            up = jnp.dot(normed[...], gu[1, :, at], preferred_element_type=jnp.float32)
            hidden[k, :, at] = (gate / (1.0 + jnp.exp(-gate)) * up).astype(jnp.bfloat16)

    def rs_copy(k, step, columns):
        return pltpu.make_async_remote_copy(
            src_ref=psend.at[k, :, columns], dst_ref=precv.at[k, :, columns],
            send_sem=rs_s.at[k, step], recv_sem=rs_r.at[k, step],
            device_id=dev(member(k), z, c), device_id_type=MESH)

    def plane_at(step):
        return (z + step * (1 - 2 * (z // (nz // 2))) + nz) % nz

    def columns_at(step):
        return pl.ds(pl.multiple_of(plane_at(step) * unit, 128), unit)

    for step in range(nz):
        zs = plane_at(step)
        if step > 0:
            @pl.when(jnp.logical_not(inner))
            def _():
                arrived(2, zs)
                to_sibling(2, zs).start()
        from_sibling(2, zs).wait_recv()
        columns = columns_at(step)
        for k in range(PLANE):
            if step == 0:
                make_hidden(k)

            @pl.loop(0, unit // 256)
            def _(j):
                at = pl.ds(pl.multiple_of(zs * unit + j * 256, 256), 256)
                part = jnp.dot(hidden[k], dn[:, at], preferred_element_type=jnp.float32)
                if k == 3:
                    own[:, at] = part
                else:
                    psend[k, :, at] = part.astype(jnp.bfloat16)

            if k < 3:
                rs_copy(k, step, columns).start()

    for step in range(nz):
        columns = columns_at(step)
        for k in range(3):
            rs_copy(k, step, columns).wait_recv()

        @pl.loop(0, unit // 256)
        def _(j):
            at = pl.ds(pl.multiple_of(plane_at(step) * unit + j * 256, 256), 256)
            total = own[:, at]
            for k in range(3):
                total = total + precv[k, :, at].astype(jnp.float32)
            out_ref[:, at] = total.astype(out_ref.dtype)

    for m in range(3):
        for k in range(3):
            a2a(m, k).wait_send()
        for zs in range(nz):
            to_sibling(m, zs).wait_send()

            @pl.when((zs <= z) & (z < nz - 1))
            def _():
                along(m, zs, 1).wait_send()

            @pl.when((zs >= z) & (z > 0))
            def _():
                along(m, zs, -1).wait_send()
    for k in range(3):
        tok_copy(k).wait_send()
        for step in range(nz):
            rs_copy(k, step, columns_at(step)).wait_send()


def fused(nfs, tokens, norm_gain, gate_weight, up_weight, down_weight):
    nz = nfs // PLANE
    features = tokens.shape[1]
    rows = tokens.shape[0] // 2
    width = gate_weight.shape[1] // PLANE
    any_spec = pl.BlockSpec(memory_space=pl.ANY)
    vmem_spec = pl.BlockSpec(memory_space=pltpu.VMEM)
    dma = pltpu.SemaphoreType.DMA
    bf16 = jnp.bfloat16
    return pl.pallas_call(
        functools.partial(kernel, nz),
        out_shape=jax.ShapeDtypeStruct((rows, features), bf16),
        in_specs=[any_spec, vmem_spec, any_spec, any_spec, any_spec],
        out_specs=vmem_spec,
        scratch_shapes=[
            pltpu.VMEM((PLANE, rows, features), bf16),
            pltpu.VMEM((rows, features), bf16),
            pltpu.VMEM((2, features, 2 * width), bf16),
            pltpu.VMEM((2 * width, features), bf16),
            pltpu.VMEM((PLANE, rows, 2 * width), bf16),
            pltpu.VMEM((3, rows, features), bf16),
            pltpu.VMEM((3, rows, features), bf16),
            pltpu.VMEM((rows, features), jnp.float32),
            dma((4,)), dma((3, 3)), dma((3, 3)), dma((3,)), dma((3,)),
            dma((3, nz)), dma((3, nz)), dma((3, nz)), dma((3, nz)), dma((3, nz)),
            dma((3, nz)), dma((3, nz)),
        ],
        compiler_params=pltpu.CompilerParams(
            collective_id=0, has_side_effects=True, vmem_limit_bytes=60 * 1024 * 1024
        ),
    )(tokens, norm_gain.reshape(1, features), gate_weight, up_weight, down_weight)


def per_device(nfs, ntp, tokens, norm_gain, gate_weight, up_weight, down_weight):
    rows, depth = tokens.shape[0] // 2, gate_weight.shape[0]
    fits = (
        ntp == 2
        and nfs % PLANE == 0
        and (nfs // PLANE) % 2 == 0
        and rows % 96 == 0
        and depth % 128 == 0
        and depth * nfs == tokens.shape[1]
        and gate_weight.shape[1] % (PLANE * 128) == 0
    )
    body = functools.partial(fused, nfs) if fits else simple
    return body(tokens, norm_gain, gate_weight, up_weight, down_weight)


def solution(mesh):
    in_specs = (P("fs", None), P(), P("fs", "tp"), P("fs", "tp"), P("tp", "fs"))
    out_specs = P(("fs", "tp"), None)
    body = functools.partial(per_device, mesh.shape["fs"], mesh.shape["tp"])
    return jax.shard_map(
        body, mesh=mesh, in_specs=in_specs, out_specs=out_specs, check_vma=False
    )
```

time: 490 us -> 212 us (0.43)
  the two profiles are of different devices: /device:TPU:1 before, /device:TPU:8 now
where the time goes in v1:
time: 212 us
  Pallas kernels  209 us (99%)
  local copies, waits for them, and re-layouts  2.73 us (1%)
    pallas_call x1, Pallas kernels, fused(): pl.pallas_call(functools.partial(kernel, nz), out_shape=jax.ShapeDtypeStr...  209 us

profile of v1, /device:TPU:8, one launch (start us, length us, event | category | flops | bytes accessed | tf_op | source)
XLA Modules:
  0.0 211.7 jit_solution(6793032143653163798)
XLA Ops:
  0.0 208.9 %shard_map.55 = bf16[384,2048]{1,0:T(8,128)(2,1)} custom-call(bf16[768,2048]{1,0:T(8,128)(2,1)} %tok_hbm.1, f32[1,2048]{1,0:T(1,128)} %bitcast.1, bf16[128,2560]{1,0:T(8,128)(2,1)} %gate_hbm.1, bf16[128,2560]{1,0:T(8,128)(2,1)} %up_hbm.1, bf16[2560,128]{1,0:T(8,128)(2,1)} %down_hbm.1), custom_call_target="tpu_custom_call" | custom-call | tf_op jit(solution)/shard_map/pallas_call | solution.py:294
  208.9 2.7 %copy.7 = bf16[384,2048]{1,0:T(8,128)(2,1)} copy(bf16[384,2048]{1,0:T(8,128)(2,1)} %shard_map.55) | data formatting | bytes 3145728

commit v2 on v1

--- a/solution.py
+++ b/solution.py
@@ -33,7 +33,7 @@
 
 def kernel(nz, tok_hbm, gain_ref, gate_hbm, up_hbm, down_hbm, out_ref,
            tok, normed, gu, dn, hidden, psend, precv, own,
-           loc_sem, a2a_s, a2a_r, tok_s, tok_r, up_s, dn_s, z_r, sib_s, sib_r, rs_s, rs_r):
+           loc_sem, a2a_s, a2a_r, tok_s, tok_r, up_s, dn_s, z_r, sib_s, sib_r, one_s, one_r, rs_s, rs_r):
     f = lax.axis_index("fs")
     c = lax.axis_index("tp")
     z, p = f // PLANE, f % PLANE
@@ -148,19 +148,41 @@
     def arrived(m, zs):
         along(m, zs, 1).wait_recv()
 
+    def piece(m, k, step):
+        ref = weight_dst(m, (z * PLANE + member(k)) * depth, depth)
+        sems = up_s if step > 0 else dn_s
+        return pltpu.make_async_remote_copy(
+            src_ref=piece_src(m, p) if k == 3 else ref, dst_ref=ref,
+            send_sem=sems.at[m, z], recv_sem=z_r.at[m, z],
+            device_id=dev(p, z + step, c), device_id_type=MESH)
+
+    def pass_piece(m, k):
+        @pl.when(z < nz - 1)
+        def _():
+            piece(m, k, 1).start()
+
+        @pl.when(z > 0)
+        def _():
+            piece(m, k, -1).start()
+
     for m in range(3):
-        for k in range(3):
+        for k in (1, 2, 0):
             a2a(m, k).start()
         local(m).start()
-    for k in range(3):
+        if m < 2:
+            pass_piece(m, 3)
+    for k in (1, 2, 0):
         tok_copy(k).start()
     own_tok.start()
 
     def own_unit(m):
+        if m == 2:
+            pass_piece(m, 3)
+        for k in (1, 2, 0):
+            a2a_in(m, k).wait_recv()
+            pass_piece(m, k)
         local(m).wait()
-        for k in range(3):
-            a2a_in(m, k).wait_recv()
-        forward(m, z)
+        to_sibling(m, z).start()
 
     own_unit(0)
     own_unit(1)
@@ -177,7 +199,8 @@
                 forward(m, z + d)
     own_unit(2)
     inner = (z > 0) & (z < nz - 1)
-    for d in range(1, nz):
+
+    def relay_down(d):
         @pl.when(inner & (z - d >= 0))
         def _():
             arrived(2, z - d)
@@ -213,10 +236,20 @@
             up = jnp.dot(normed[...], gu[1, :, at], preferred_element_type=jnp.float32)
             hidden[k, :, at] = (gate / (1.0 + jnp.exp(-gate)) * up).astype(jnp.bfloat16)
 
-    def rs_copy(k, step, columns):
-        return pltpu.make_async_remote_copy(
-            src_ref=psend.at[k, :, columns], dst_ref=precv.at[k, :, columns],
-            send_sem=rs_s.at[k, step], recv_sem=rs_r.at[k, step],
+    part_rows = (pl.ds(0, rows // 2), pl.ds(rows // 2, rows // 2))
+
+    def first(h, step):
+        at = (0, part_rows[h], columns_at(step))
+        return pltpu.make_async_remote_copy(
+            src_ref=psend.at[at], dst_ref=precv.at[at],
+            send_sem=one_s.at[h, step], recv_sem=one_r.at[h, step],
+            device_id=dev(member(1 + h), z, c), device_id_type=MESH)
+
+    def last(k, h, step):
+        at = (k, part_rows[h], columns_at(step))
+        return pltpu.make_async_remote_copy(
+            src_ref=psend.at[at], dst_ref=precv.at[at],
+            send_sem=rs_s.at[2 * k + h - 2, step], recv_sem=rs_r.at[2 * k + h - 2, step],
             device_id=dev(member(k), z, c), device_id_type=MESH)
 
     def plane_at(step):
@@ -224,6 +257,16 @@
 
     def columns_at(step):
         return pl.ds(pl.multiple_of(plane_at(step) * unit, 128), unit)
+
+    def add_and_send(step):
+        for h in range(2):
+            k = 2 - h
+            first(h, step).wait_recv()
+            at = (part_rows[h], columns_at(step))
+            psend[(k, *at)] = (
+                psend[(k, *at)].astype(jnp.float32) + precv[(0, *at)].astype(jnp.float32)
+            ).astype(jnp.bfloat16)
+            last(k, h, step).start()
 
     for step in range(nz):
         zs = plane_at(step)
@@ -232,8 +275,9 @@
             def _():
                 arrived(2, zs)
                 to_sibling(2, zs).start()
+
+            relay_down(step)
         from_sibling(2, zs).wait_recv()
-        columns = columns_at(step)
         for k in range(PLANE):
             if step == 0:
                 make_hidden(k)
@@ -247,19 +291,27 @@
                 else:
                     psend[k, :, at] = part.astype(jnp.bfloat16)
 
-            if k < 3:
-                rs_copy(k, step, columns).start()
+            if k == 0:
+                first(0, step).start()
+                first(1, step).start()
+            elif k < 3:
+                last(k, k - 1, step).start()
+        if step == 0:
+            add_and_send(0)
+        elif step > 1:
+            add_and_send(step - 1)
+    add_and_send(nz - 1)
 
     for step in range(nz):
-        columns = columns_at(step)
-        for k in range(3):
-            rs_copy(k, step, columns).wait_recv()
+        for k in (1, 2):
+            for h in range(2):
+                last(k, h, step).wait_recv()
 
         @pl.loop(0, unit // 256)
         def _(j):
             at = pl.ds(pl.multiple_of(plane_at(step) * unit + j * 256, 256), 256)
             total = own[:, at]
-            for k in range(3):
+            for k in (1, 2):
                 total = total + precv[k, :, at].astype(jnp.float32)
             out_ref[:, at] = total.astype(out_ref.dtype)
 
@@ -278,8 +330,11 @@
                 along(m, zs, -1).wait_send()
     for k in range(3):
         tok_copy(k).wait_send()
-        for step in range(nz):
-            rs_copy(k, step, columns_at(step)).wait_send()
+    for step in range(nz):
+        for h in range(2):
+            first(h, step).wait_send()
+            for k in (1, 2):
+                last(k, h, step).wait_send()
 
 
 def fused(nfs, tokens, norm_gain, gate_weight, up_weight, down_weight):
@@ -307,7 +362,7 @@
             pltpu.VMEM((rows, features), jnp.float32),
             dma((4,)), dma((3, 3)), dma((3, 3)), dma((3,)), dma((3,)),
             dma((3, nz)), dma((3, nz)), dma((3, nz)), dma((3, nz)), dma((3, nz)),
-            dma((3, nz)), dma((3, nz)),
+            dma((2, nz)), dma((2, nz)), dma((4, nz)), dma((4, nz)),
         ],
         compiler_params=pltpu.CompilerParams(
             collective_id=0, has_side_effects=True, vmem_limit_bytes=60 * 1024 * 1024

time: 212 us -> 178 us (0.84)
  the two profiles are of different devices: /device:TPU:8 before, /device:TPU:1 now
where the time goes in v2:
time: 178 us
  Pallas kernels  175 us (98%)
  local copies, waits for them, and re-layouts  2.73 us (2%)
    pallas_call x1, Pallas kernels, fused(): pl.pallas_call(functools.partial(kernel, nz), out_shape=jax.ShapeDtypeStr...  175 us

profile of v2, /device:TPU:1, one launch (start us, length us, event | category | flops | bytes accessed | tf_op | source)
XLA Modules:
  0.0 178.0 jit_solution(15161731009446758451)
XLA Ops:
  0.0 175.2 %shard_map.55 = bf16[384,2048]{1,0:T(8,128)(2,1)} custom-call(bf16[768,2048]{1,0:T(8,128)(2,1)} %tok_hbm.1, f32[1,2048]{1,0:T(1,128)} %bitcast.1, bf16[128,2560]{1,0:T(8,128)(2,1)} %gate_hbm.1, bf16[128,2560]{1,0:T(8,128)(2,1)} %up_hbm.1, bf16[2560,128]{1,0:T(8,128)(2,1)} %down_hbm.1), custom_call_target="tpu_custom_call" | custom-call | tf_op jit(solution)/shard_map/pallas_call | solution.py:349
  175.2 2.7 %copy.7 = bf16[384,2048]{1,0:T(8,128)(2,1)} copy(bf16[384,2048]{1,0:T(8,128)(2,1)} %shard_map.55) | data formatting | bytes 3145728

commit v3 on v2

--- a/solution.py
+++ b/solution.py
@@ -32,7 +32,7 @@
 
 
 def kernel(nz, tok_hbm, gain_ref, gate_hbm, up_hbm, down_hbm, out_ref,
-           tok, normed, gu, dn, hidden, psend, precv, own,
+           tok, acc, gu, dn, hidden, psend, precv, own,
            loc_sem, a2a_s, a2a_r, tok_s, tok_r, up_s, dn_s, z_r, sib_s, sib_r, one_s, one_r, rs_s, rs_r):
     f = lax.axis_index("fs")
     c = lax.axis_index("tp")
@@ -186,7 +186,7 @@
 
     own_unit(0)
     own_unit(1)
-    for d in range(1, nz):
+    def relay_wide(d):
         for m in range(2):
             @pl.when(z - d >= 0)
             def _():
@@ -197,6 +197,8 @@
             def _():
                 arrived(m, z + d)
                 forward(m, z + d)
+    for d in range(1, nz - 1):
+        relay_wide(d)
     own_unit(2)
     inner = (z > 0) & (z < nz - 1)
 
@@ -211,11 +213,17 @@
             arrived(2, z + d)
             forward(2, z + d)
 
+    end = z // (nz - 1)
+    late = (nz - 1) * (1 - end)
+
+    def project(m, k, at, start, size):
+        depths = pl.ds(pl.multiple_of(start * unit, 128), size * unit)
+        return jnp.dot(tok[k, :, depths], gu[m, depths, at], preferred_element_type=jnp.float32)
+
     for m in range(2):
-        for zs in range(nz):
-            from_sibling(m, zs).wait_recv()
-
-    def make_hidden(k):
+        for i in range(nz - 1):
+            from_sibling(m, end + i).wait_recv()
+    for k in (3, 1, 2, 0):
         if k == 3:
             own_tok.wait()
         else:
@@ -227,13 +235,24 @@
             at = pl.ds(pl.multiple_of(i * block, 16), block)
             values = tok[k, at, :].astype(jnp.float32)
             scale = lax.rsqrt(jnp.mean(values * values, axis=-1, keepdims=True) + 1e-06)
-            normed[at, :] = (values * scale * gain_ref[...]).astype(jnp.bfloat16)
+            tok[k, at, :] = (values * scale * gain_ref[...]).astype(jnp.bfloat16)
 
         @pl.loop(0, 2 * width // 256)
         def _(j):
             at = pl.ds(pl.multiple_of(j * 256, 256), 256)
-            gate = jnp.dot(normed[...], gu[0, :, at], preferred_element_type=jnp.float32)
-            up = jnp.dot(normed[...], gu[1, :, at], preferred_element_type=jnp.float32)
+            for m in range(2):
+                acc[m, k, :, at] = project(m, k, at, end, nz - 1)
+
+    relay_wide(nz - 1)
+    for m in range(2):
+        from_sibling(m, late).wait_recv()
+
+    def make_hidden(k):
+        @pl.loop(0, 2 * width // 256)
+        def _(j):
+            at = pl.ds(pl.multiple_of(j * 256, 256), 256)
+            gate = acc[0, k, :, at] + project(0, k, at, late, 1)
+            up = acc[1, k, :, at] + project(1, k, at, late, 1)
             hidden[k, :, at] = (gate / (1.0 + jnp.exp(-gate)) * up).astype(jnp.bfloat16)
 
     part_rows = (pl.ds(0, rows // 2), pl.ds(rows // 2, rows // 2))
@@ -353,7 +372,7 @@
         out_specs=vmem_spec,
         scratch_shapes=[
             pltpu.VMEM((PLANE, rows, features), bf16),
-            pltpu.VMEM((rows, features), bf16),
+            pltpu.VMEM((2, PLANE, rows, 2 * width), jnp.float32),
             pltpu.VMEM((2, features, 2 * width), bf16),
             pltpu.VMEM((2 * width, features), bf16),
             pltpu.VMEM((PLANE, rows, 2 * width), bf16),
@@ -365,7 +384,7 @@
             dma((2, nz)), dma((2, nz)), dma((4, nz)), dma((4, nz)),
         ],
         compiler_params=pltpu.CompilerParams(
-            collective_id=0, has_side_effects=True, vmem_limit_bytes=60 * 1024 * 1024
+            collective_id=0, has_side_effects=True, vmem_limit_bytes=62 * 1024 * 1024
         ),
     )(tokens, norm_gain.reshape(1, features), gate_weight, up_weight, down_weight)
 

time: 178 us -> 167 us (0.938)
  Pallas kernels: 175 us -> 164 us
    pallas_call x1, Pallas kernels: 175 us -> 164 us  [fused(): pl.pallas_call(functools.partial(kernel, nz), out_shape=jax.ShapeDtypeStr...]
where the time goes in v3:
time: 167 us
  Pallas kernels  164 us (98%)
  local copies, waits for them, and re-layouts  2.73 us (2%)
    pallas_call x1, Pallas kernels, fused(): pl.pallas_call(functools.partial(kernel, nz), out_shape=jax.ShapeDtypeStr...  164 us

profile of v3, /device:TPU:1, one launch (start us, length us, event | category | flops | bytes accessed | tf_op | source)
XLA Modules:
  0.0 167.1 jit_solution(2477939148938982099)
XLA Ops:
  0.0 164.4 %shard_map.55 = bf16[384,2048]{1,0:T(8,128)(2,1)} custom-call(bf16[768,2048]{1,0:T(8,128)(2,1)} %tok_hbm.1, f32[1,2048]{1,0:T(1,128)} %bitcast.1, bf16[128,2560]{1,0:T(8,128)(2,1)} %gate_hbm.1, bf16[128,2560]{1,0:T(8,128)(2,1)} %up_hbm.1, bf16[2560,128]{1,0:T(8,128)(2,1)} %down_hbm.1), custom_call_target="tpu_custom_call" | custom-call | tf_op jit(solution)/shard_map/pallas_call | solution.py:368
  164.4 2.7 %copy.7 = bf16[384,2048]{1,0:T(8,128)(2,1)} copy(bf16[384,2048]{1,0:T(8,128)(2,1)} %shard_map.55) | data formatting | bytes 3145728
